TPU v7x, 32 devices: a whole 2x2x4 slice. The times are simulated.
32 devices in a mesh: kv: 8 (over z, y), tp: 4 (over x, core).
Axes of the slice: x: 2, y: 2, z: 4, core: 2. Of those that a mesh axis runs over, the one named last changes fastest.
Arguments:
- tokens: bfloat16 [4096, 2048], P('kv', 'tp'), may hold values from -9 to 9
- w_query: bfloat16 [2048, 1536], P(None, 'tp'), may hold values from -1 to 1
- w_key: bfloat16 [2048, 1536], P(None, 'tp'), may hold values from -1 to 1
- w_value: bfloat16 [2048, 1536], P(None, 'tp'), may hold values from -0.5 to 0.5
- w_out: bfloat16 [1536, 2048], P('tp'), may hold values from -0.15625 to 0.15625
- chosen: int32 [128, 24], P('kv'), may hold values from 0 to 127, as said below
Outputs:
- mixed: bfloat16 [4096, 2048], P(('kv', 'tp'))
Inputs may be any that keep to these rules, and one draw needn't show every extreme that they name: `chosen`: row c names blocks no later than c; its first entry is c and its second c - 1 (0 for row 0), and an entry may repeat. Taking the rows in aligned runs of 16, one run for each index of kv, the rows of one run name at most 2 distinct blocks lying in any one other index's positions; in every draw some index of kv names exactly 2 from every earlier index. Every run names some block of the index just before it and of the index half the axis before it, where those exist.
All inputs are finite; a program needn't handle non-finite values.
Results may differ from a plain program's by a relative error of at most 0.014.
Values may be sent and summed in bfloat16 or wider, within the bound.
A program may use at most 320 MiB of HBM per device.

v0:
```python
import jax
import jax.numpy as jnp
from jax import lax
from jax.sharding import PartitionSpec as P

HD = 128
BLK = 32
MOST = 2
NEG = -1e30


def attend(query_rows, key_rows, value_rows, block_ids, chosen, first_block):
    tok_rows, width = query_rows.shape
    head_count = width // HD
    key_count = key_rows.shape[0]
    slot_count = key_count // BLK
    query_blocks = tok_rows // BLK
    seen = (
        jnp.any(chosen[:, :, None] == block_ids[None, None, :], axis=1) & (block_ids >= 0)[None, :]
    )
    grid = jnp.broadcast_to(seen[:, None, :, None], (query_blocks, BLK, slot_count, BLK)).reshape(
        tok_rows, key_count
    )
    key_pos = (block_ids[:, None] * BLK + jnp.arange(BLK, dtype=jnp.int32)[None, :]).reshape(
        key_count
    )
    query_pos = first_block * BLK + jnp.arange(tok_rows, dtype=jnp.int32)
    allowed = grid & (key_pos[None, :] <= query_pos[:, None])
    query_heads = query_rows.reshape(tok_rows, head_count, HD)
    key_heads = key_rows.reshape(key_count, head_count, HD)
    value_heads = value_rows.reshape(key_count, head_count, HD)
    scores = jnp.einsum(
        "qhd,khd->hqk", query_heads, key_heads, preferred_element_type=jnp.float32
    ) * HD ** (-0.5)
    scores = jnp.where(allowed[None], scores, NEG)
    highest = jnp.max(scores, axis=-1)
    weights = jnp.where(allowed[None], jnp.exp(scores - highest[..., None]), 0.0)
    totals = jnp.sum(weights, axis=-1)
    summed = jnp.einsum("hqk,khd->hqd", weights, value_heads.astype(jnp.float32))
    return (highest, totals, summed)


def combine(left, right):
    highest = jnp.maximum(left[0], right[0])
    left_scale = jnp.exp(left[0] - highest)
    right_scale = jnp.exp(right[0] - highest)
    totals = left[1] * left_scale + right[1] * right_scale
    summed = left[2] * left_scale[..., None] + right[2] * right_scale[..., None]
    return (highest, totals, summed)


def local(tokens, w_query, w_key, w_value, w_out, chosen):
    tok_rows = tokens.shape[0]
    width = w_query.shape[1]
    empty = jnp.zeros((tok_rows, width), jnp.float32)
    totals = (empty, empty, empty)
    piece = lax.all_gather(tokens, "tp", axis=1, tiled=True)
    outputs = []
    for total, weight in zip(totals, (w_query, w_key, w_value)):
        rows = weight
        outputs.append(jnp.dot(piece, rows, preferred_element_type=jnp.float32))
    query_full, key_full, value_full = tuple(outputs)
    query_rows = query_full.astype(jnp.bfloat16)
    key_rows = key_full.astype(jnp.bfloat16)
    value_rows = value_full.astype(jnp.bfloat16)
    per_dev = tok_rows // BLK
    my_index = lax.axis_index("kv")
    first_block = my_index * per_dev
    own_ids = first_block + jnp.arange(per_dev, dtype=jnp.int32)
    own_part = attend(query_rows, key_rows, value_rows, own_ids, chosen, first_block)
    peers = lax.axis_size("kv")
    block_total = peers * per_dev
    wanted = jnp.any(
        chosen[:, :, None] == jnp.arange(block_total, dtype=jnp.int32)[None, None, :], axis=(0, 1)
    )
    peer_ids = jnp.arange(peers, dtype=jnp.int32)
    wanted = wanted.reshape(peers, per_dev) & (peer_ids != my_index)[:, None]
    ranks = jnp.cumsum(wanted.astype(jnp.int32), axis=1) - 1
    slot_hit = wanted[:, :, None] & (
        ranks[:, :, None] == jnp.arange(MOST, dtype=jnp.int32)[None, None, :]
    )
    local_ids = jnp.sum(
        slot_hit.astype(jnp.int32) * jnp.arange(per_dev, dtype=jnp.int32)[None, :, None], axis=1
    )
    present = jnp.any(slot_hit, axis=1)
    request = jnp.where(present, local_ids, -1)
    asked = lax.all_to_all(request, "kv", split_axis=0, concat_axis=0, tiled=True)
    picked = jnp.clip(asked, 0).reshape(-1)
    send_keys = key_rows.reshape(per_dev, BLK, width)[picked]
    send_values = value_rows.reshape(per_dev, BLK, width)[picked]
    got_keys, got_values = (
        lax.all_to_all(send_keys, "kv", split_axis=0, concat_axis=0, tiled=True),
        lax.all_to_all(send_values, "kv", split_axis=0, concat_axis=0, tiled=True),
    )
    got_ids = jnp.where(present, peer_ids[:, None] * per_dev + local_ids, -1).reshape(-1)
    far_part = attend(
        query_rows,
        got_keys.reshape(-1, width),
        got_values.reshape(-1, width),
        got_ids,
        chosen,
        first_block,
    )
    merged = combine(own_part, far_part)
    normed = merged[2] / merged[1][..., None]
    attended = jnp.transpose(normed, (1, 0, 2)).reshape(tok_rows, width).astype(jnp.bfloat16)
    rows = attended
    return lax.psum_scatter(
        jnp.dot(rows, w_out, preferred_element_type=jnp.float32).astype(jnp.bfloat16),
        "tp",
        scatter_dimension=0,
        tiled=True,
    )


def solution(mesh):
    return jax.shard_map(
        local,
        mesh=mesh,
        in_specs=(
            P("kv", "tp"),
            P(None, "tp"),
            P(None, "tp"),
            P(None, "tp"),
            P("tp", None),
            P("kv", None),
        ),
        out_specs=P(("kv", "tp"), None),
        check_vma=False,
    )
```

profile of v0, /device:TPU:0, one launch (start us, length us, event | category | flops | bytes accessed | tf_op | source)
XLA Modules:
  0.0 118.5 jit_solution(13071488536581529827)
XLA Ops:
  6.5 0.0 copy-start
  6.5 0.0 all-gather.2.cloned.1.call-start
  6.5 0.7 all-gather.2.cloned.1.call-update
  7.3 0.8 fusion.26
  8.1 0.1 reshape.337
  8.2 0.1 fusion.40
  8.3 0.2 reduce_window_sum.11
  8.4 0.2 fusion.31
  8.6 0.2 select_reduce_fusion
  8.8 0.7 copy.46
  9.4 7.3 %all-to-all-start = ((s32[8,1,2]{2,1,0:T(1,128)}), s32[8,1,2]{2,1,0:T(1,128)S(1)}, u32[]{:S(2)}, u32[]{:S(2)}) async-start(s32[8,1,2]{2,1,0:T(1,128)} %copy.46), calls=%async_computation | async-start | bytes 8192 | tf_op jit(solution)/shard_map/all_to_all | solution.py:87
  16.7 0.1 copy.44
  16.8 0.1 select_n.53
  16.9 1.4 %compare_reduce_fusion = (pred[16,16]{1,0:T(8,128)(4,1)S(1)}, pred[16,16]{1,0:T(8,128)(4,1)S(1)}) fusion(s32[16,24]{1,0:T(8,128)} %param.11, s32[16]{0:T(128)S(1)} %select_n.53, s32[16]{0:T(128)S(1)} %get-tuple-element.20), kind=kLoop, calls=%fused_computation.40 | loop fusion | flops 24064 | bytes 2176 | tf_op jit(solution)/shard_map/reduce_or | solution.py:19
  18.3 0.1 copy.45
  18.4 0.3 broadcast_in_dim.42
  18.8 2.1 %reshape.338 = pred[512,512]{0,1:T(8,128)(4,1)S(1)} reshape(pred[16,32,16,32]{1,0,3,2:T(8,128)(4,1)S(1)} %broadcast_in_dim.42) | data formatting | bytes 524288 | tf_op jit(solution)/shard_map/reshape | solution.py:21
  20.9 0.1 iota_add_fusion
  21.0 0.1 add.128
  21.1 0.1 copy.38
  21.2 0.3 broadcast_in_dim.37
  21.5 2.1 %reshape.333 = pred[512,512]{0,1:T(8,128)(4,1)S(1)} reshape(pred[16,32,16,32]{1,0,3,2:T(8,128)(4,1)S(1)} %broadcast_in_dim.37) | data formatting | bytes 524288 | tf_op jit(solution)/shard_map/reshape | solution.py:21
  23.6 0.1 iota_add_fusion.1
  23.7 0.1 add.120
  23.8 0.5 compare_and_fusion
  24.3 0.0 all-to-all-done
  24.3 0.1 reshape.343
  24.4 9.8 %all-gather.2.cloned.1.call-done = bf16[512,2048]{1,0:T(8,128)(2,1)} async-done(((bf16[512,512]{1,0:T(8,128)(2,1)}), bf16[512,2048]{1,0:T(8,128)(2,1)}) %all-gather.2.cloned.1.call-update) | async-done | bytes 2097168 | tf_op jit(solution)/shard_map/all_gather | solution.py:57
  34.2 3.3 %convolution_convert_fusion.1 = bf16[512,384]{1,0:T(8,128)(2,1)S(1)} fusion(bf16[512,2048]{1,0:T(8,128)(2,1)} %all-gather.2.cloned.1.call-done, bf16[2048,384]{1,0:T(8,128)(2,1)} %param.9), kind=kOutput, calls=%fused_computation.28 | convolution fusion | flops 805502976 | bytes 4063232 | tf_op jit(solution)/shard_map/dot_general | solution.py:61
  37.5 0.9 copy.42
  38.4 3.3 %convolution_convert_fusion.2 = bf16[512,384]{1,0:T(8,128)(2,1)S(1)} fusion(bf16[512,2048]{1,0:T(8,128)(2,1)} %all-gather.2.cloned.1.call-done, bf16[2048,384]{1,0:T(8,128)(2,1)} %param.8), kind=kOutput, calls=%fused_computation.29 | convolution fusion | flops 805502976 | bytes 4063232 | tf_op jit(solution)/shard_map/dot_general | solution.py:61
  41.7 0.2 copy.39
  41.9 1.3 %gather_fusion = bf16[16,32,384]{2,1,0:T(8,128)(2,1)} fusion(bf16[16,32,384]{2,1,0:T(8,128)(2,1)S(1)} %bitcast.62, s32[1024]{0:T(1024)S(1)} %pad_clamp_fusion), kind=kCustom, calls=%fused_computation | custom fusion | bytes 786496 | tf_op jit(solution)/shard_map/gather | solution.py:89
  43.3 5.5 %all-to-all-start.1 = ((bf16[16,32,384]{2,1,0:T(8,128)(2,1)}), bf16[16,32,384]{2,1,0:T(8,128)(2,1)S(1)}, u32[]{:S(2)}, u32[]{:S(2)}) async-start(bf16[16,32,384]{2,1,0:T(8,128)(2,1)} %gather_fusion), calls=%async_computation.1 | async-start | bytes 786432 | tf_op jit(solution)/shard_map/all_to_all | solution.py:92
  48.8 1.4 %gather_fusion.1 = bf16[16,32,384]{2,1,0:T(8,128)(2,1)} fusion(bf16[16,32,384]{2,1,0:T(8,128)(2,1)S(1)} %bitcast.61, s32[1024]{0:T(1024)S(1)} %pad_clamp_fusion), kind=kCustom, calls=%fused_computation.1 | custom fusion | bytes 786496 | tf_op jit(solution)/shard_map/gather | solution.py:90
  50.2 3.1 %convolution_convert_fusion.3 = bf16[512,384]{0,1:T(8,128)(2,1)S(1)} fusion(bf16[512,2048]{1,0:T(8,128)(2,1)} %all-gather.2.cloned.1.call-done, bf16[2048,384]{1,0:T(8,128)(2,1)} %param.7), kind=kOutput, calls=%fused_computation.30 | convolution fusion | flops 805502976 | bytes 4063232 | tf_op jit(solution)/shard_map/dot_general | solution.py:61
  53.2 0.0 copy-start.4
  53.2 0.8 fusion
  54.0 0.0 copy-start.1
  54.1 1.7 %copy-done.1 = f32[3,512,512]{1,2,0:T(8,128)} copy-done((f32[3,512,512]{1,2,0:T(8,128)}, f32[3,512,512]{1,2,0:T(8,128)S(1)}, u32[]{:S(2)}) %copy-start.1) | copy-done | bytes 3145752
  55.7 0.8 fusion.2
  56.5 4.3 %all-to-all-done.1 = bf16[16,32,384]{2,1,0:T(8,128)(2,1)S(1)} async-done(((bf16[16,32,384]{2,1,0:T(8,128)(2,1)}), bf16[16,32,384]{2,1,0:T(8,128)(2,1)S(1)}, u32[]{:S(2)}, u32[]{:S(2)}) %all-to-all-start.1) | async-done | bytes 393248 | tf_op jit(solution)/shard_map/all_to_all | solution.py:92
  60.9 3.6 %all-to-all-start.2 = ((bf16[16,32,384]{2,1,0:T(8,128)(2,1)}), bf16[16,32,384]{2,1,0:T(8,128)(2,1)S(1)}, u32[]{:S(2)}, u32[]{:S(2)}) async-start(bf16[16,32,384]{2,1,0:T(8,128)(2,1)} %gather_fusion.1), calls=%async_computation.2 | async-start | bytes 786432 | tf_op jit(solution)/shard_map/all_to_all | solution.py:93
  64.5 0.0 copy-done.4
  64.5 0.2 reduce-scatter.2.cloned.1.call-start
  64.7 0.1 reshape_reshape.6
  64.8 0.0 copy-start.2
  64.9 0.0 copy-start.5
  64.9 1.9 %fusion.1 = (f32[3,512]{1,0:T(4,128)S(1)}, f32[3,512,512]{1,2,0:T(8,128)S(1)}) fusion(pred[512,512]{0,1:T(8,128)(4,1)S(1)} %get-tuple-element.12, bf16[512,3,128]{0,2,1:T(8,128)(2,1)} %bitcast.64, bf16[512,3,128]{2,1,0:T(4,128)(2,1)S(1)} %reshape_reshape.6), kind=kOutput, calls=%fused_computation.8 | convolution fusion | flops 203684352 | bytes 4200448 | tf_op jit(solution)/shard_map/qhd,khd->hqk/dot_general | solution.py:32
  66.8 0.0 copy-start.3
  66.8 1.7 %copy-done.3 = f32[3,512,512]{1,2,0:T(8,128)} copy-done((f32[3,512,512]{1,2,0:T(8,128)}, f32[3,512,512]{1,2,0:T(8,128)S(1)}, u32[]{:S(2)}) %copy-start.3) | copy-done | bytes 3145752
  68.5 0.8 fusion.4
  69.3 0.0 copy-done.2
  69.3 0.0 copy-done.5
  69.3 1.9 %fusion.18 = f32[512,3,128]{0,2,1:T(8,128)} fusion(bf16[512,3,128]{0,2,1:T(8,128)(2,1)S(1)} %bitcast.65, f32[3,512,512]{1,2,0:T(8,128)S(1)} %copy-done.2, f32[3,512]{1,0:T(4,128)S(1)} %get-tuple-element.16, pred[512,512]{0,1:T(8,128)(4,1)S(1)} %get-tuple-element.13, f32[512,3]{0,1:T(4,128)S(1)} %get-tuple-element.9), kind=kOutput, calls=%fused_computation.25 | convolution fusion | flops 204668928 | bytes 4599808 | tf_op jit(solution)/shard_map/hqk,khd->hqd/dot_general | solution.py:39
  71.2 5.2 %all-to-all-done.2 = bf16[16,32,384]{2,1,0:T(8,128)(2,1)S(1)} async-done(((bf16[16,32,384]{2,1,0:T(8,128)(2,1)}), bf16[16,32,384]{2,1,0:T(8,128)(2,1)S(1)}, u32[]{:S(2)}, u32[]{:S(2)}) %all-to-all-start.2) | async-done | bytes 393248 | tf_op jit(solution)/shard_map/all_to_all | solution.py:93
  76.4 0.1 reshape_reshape.7
  76.5 3.1 %fusion.22 = bf16[512,3,128]{0,2,1:T(8,128)(2,1)S(1)} fusion(f32[512,3,128]{0,2,1:T(8,128)} %fusion.18, f32[3,512,512]{1,2,0:T(8,128)} %copy-done.3, f32[3,512]{1,0:T(4,128)S(1)} %get-tuple-element.18, pred[512,512]{0,1:T(8,128)(4,1)S(1)} %get-tuple-element.12, bf16[512,3,128]{2,1,0:T(4,128)(2,1)S(1)} %reshape_reshape.7, ...), kind=kOutput, calls=%fused_computation.34 | convolution fusion | flops 205258752 | bytes 4999168 | tf_op jit(solution)/shard_map/hqk,khd->hqd/dot_general | solution.py:39
  79.6 0.0 copy-done
  79.6 2.7 %convolution_convert_fusion = bf16[512,2048]{1,0:T(8,128)(2,1)} fusion(bf16[512,384]{0,1:T(8,128)(2,1)S(1)} %bitcast.66, bf16[384,2048]{1,0:T(8,128)(2,1)S(1)} %copy-done), kind=kOutput, calls=%fused_computation.6 | convolution fusion | flops 806354944 | bytes 4063232 | tf_op jit(solution)/shard_map/dot_general | solution.py:109
  82.2 0.0 reduce-scatter.2.cloned.1.call-update
  82.3 29.4 %reduce-scatter.2.cloned.1.call-done = bf16[128,2048]{1,0:T(8,128)(2,1)} async-done(((bf16[512,2048]{1,0:T(8,128)(2,1)}), bf16[128,2048]{1,0:T(8,128)(2,1)}) %reduce-scatter.2.cloned.1.call-update) | async-done | bytes 524304 | tf_op jit(solution)/shard_map/reduce_scatter | solution.py:108
  (14 shorter events, 0.1 us)
Async XLA Ops:
  6.5 73.0 %copy-start = (bf16[384,2048]{1,0:T(8,128)(2,1)S(1)}, bf16[384,2048]{1,0:T(8,128)(2,1)}, u32[]{:S(2)}) copy-start(bf16[384,2048]{1,0:T(8,128)(2,1)} %param.10) | copy-start | bytes 4718596
  6.5 27.7 %all-gather.2.cloned.1.call-start = ((), (), s32[]{:S(2)}) async-start(), calls=%async_computation.4 | async-start | bytes 2621440 | tf_op jit(solution)/shard_map/all_gather | solution.py:57
  9.4 14.8 %all-to-all-start = ((s32[8,1,2]{2,1,0:T(1,128)}), s32[8,1,2]{2,1,0:T(1,128)S(1)}, u32[]{:S(2)}, u32[]{:S(2)}) async-start(s32[8,1,2]{2,1,0:T(1,128)} %copy.46), calls=%async_computation | async-start | bytes 8192 | tf_op jit(solution)/shard_map/all_to_all | solution.py:87
  43.3 17.6 %all-to-all-start.1 = ((bf16[16,32,384]{2,1,0:T(8,128)(2,1)}), bf16[16,32,384]{2,1,0:T(8,128)(2,1)S(1)}, u32[]{:S(2)}, u32[]{:S(2)}) async-start(bf16[16,32,384]{2,1,0:T(8,128)(2,1)} %gather_fusion), calls=%async_computation.1 | async-start | bytes 786432 | tf_op jit(solution)/shard_map/all_to_all | solution.py:92
  53.2 11.3 %copy-start.4 = (bf16[512,384]{0,1:T(8,128)(2,1)}, bf16[512,384]{0,1:T(8,128)(2,1)S(1)}, u32[]{:S(2)}) copy-start(bf16[512,384]{0,1:T(8,128)(2,1)S(1)} %convolution_convert_fusion.3) | copy-start | bytes 1179652
  54.0 1.7 %copy-start.1 = (f32[3,512,512]{1,2,0:T(8,128)}, f32[3,512,512]{1,2,0:T(8,128)S(1)}, u32[]{:S(2)}) copy-start(f32[3,512,512]{1,2,0:T(8,128)S(1)} %get-tuple-element.17) | copy-start | bytes 9437188
  60.9 15.5 %all-to-all-start.2 = ((bf16[16,32,384]{2,1,0:T(8,128)(2,1)}), bf16[16,32,384]{2,1,0:T(8,128)(2,1)S(1)}, u32[]{:S(2)}, u32[]{:S(2)}) async-start(bf16[16,32,384]{2,1,0:T(8,128)(2,1)} %gather_fusion.1), calls=%async_computation.2 | async-start | bytes 786432 | tf_op jit(solution)/shard_map/all_to_all | solution.py:93
  64.5 47.2 %reduce-scatter.2.cloned.1.call-start = ((), (), s32[]{:S(2)}) async-start(), calls=%async_computation.5 | async-start | bytes 2621440 | tf_op jit(solution)/shard_map/reduce_scatter | solution.py:108
  64.8 4.5 %copy-start.2 = (f32[3,512,512]{1,2,0:T(8,128)S(1)}, f32[3,512,512]{1,2,0:T(8,128)}, u32[]{:S(2)}) copy-start(f32[3,512,512]{1,2,0:T(8,128)} %copy-done.1) | copy-start | bytes 9437188
  64.9 4.5 %copy-start.5 = (bf16[512,384]{0,1:T(8,128)(2,1)S(1)}, bf16[512,384]{0,1:T(8,128)(2,1)}, u32[]{:S(2)}) copy-start(bf16[512,384]{0,1:T(8,128)(2,1)} %copy.42) | copy-start | bytes 1179652
  66.8 1.7 %copy-start.3 = (f32[3,512,512]{1,2,0:T(8,128)}, f32[3,512,512]{1,2,0:T(8,128)S(1)}, u32[]{:S(2)}) copy-start(f32[3,512,512]{1,2,0:T(8,128)S(1)} %get-tuple-element.19) | copy-start | bytes 9437188
Sparse Core Ops, SparseCore 0:
  8.9 25.2 all-gather.1
  82.4 29.2 reduce-scatter.1
where the time goes:
time: 119 us
  waiting for transfers between devices  49.5 us (42%)
  matrix products  19.9 us (17%)
  starting transfers between devices  16.7 us (14%)
  local copies, waits for them, and re-layouts  13.7 us (12%)
  between operations  13.6 us (11%)
  other arithmetic  5.12 us (4%)
    reduce_scatter x1, waiting for transfers between devices, local(): lax.psum_scatter(jnp.dot(rows, w_out, preferred_element_type=jnp.float32)...  29.4 us
    all_gather x1, waiting for transfers between devices, local(): piece = lax.all_gather(tokens, 'tp', axis=1, tiled=True)  9.83 us
    dot_general x3, matrix products, local(): outputs.append(jnp.dot(piece, rows, preferred_element_type=jnp.float32))  9.62 us
    all_to_all x1, starting transfers between devices, local(): lax.all_to_all(request, 'kv', split_axis=0, concat_axis=0, tiled=True)  7.31 us
    all_to_all x1, starting transfers between devices, local(): lax.all_to_all(send_keys, 'kv', split_axis=0, concat_axis=0, tiled=True)  5.51 us
    all_to_all x1, waiting for transfers between devices, local(): lax.all_to_all(send_values, 'kv', split_axis=0, concat_axis=0, tiled=True)  5.16 us
    dot_general x2, matrix products, attend(): jnp.einsum('hqk,khd->hqd', weights, value_heads.astype(jnp.float32))  4.96 us
    all_to_all x1, waiting for transfers between devices, local(): lax.all_to_all(send_keys, 'kv', split_axis=0, concat_axis=0, tiled=True)  4.32 us
  transfers between devices with their start and end apart: 5, of which 4 were waited for; matrix products, arithmetic and copies ran while one was open for 17% of the time, Pallas kernels for 0%

commit v1 on v0

--- a/solution.py
+++ b/solution.py
@@ -54,7 +54,13 @@
     width = w_query.shape[1]
     empty = jnp.zeros((tok_rows, width), jnp.float32)
     totals = (empty, empty, empty)
-    piece = lax.all_gather(tokens, "tp", axis=1, tiled=True)
+    n_dev = lax.axis_size("tp")
+    held, blocks = (tokens, [tokens])
+    for _ in range(n_dev - 1):
+        held = lax.ppermute(held, "tp", [(i, (i + 1) % n_dev) for i in range(n_dev)])
+        blocks.insert(0, held)
+    row_of_blocks = jnp.concatenate(blocks, axis=1)
+    piece = jnp.roll(row_of_blocks, (lax.axis_index("tp") + 1) * tokens.shape[1], axis=1)
     outputs = []
     for total, weight in zip(totals, (w_query, w_key, w_value)):
         rows = weight

time: 119 us -> 135 us (1.13)
  local copies, waits for them, and re-layouts: 13.7 us -> 25.6 us
  starting transfers between devices: 16.7 us -> 18.6 us
  other arithmetic: 5.12 us -> 6.76 us
    unnamed x12 -> x31, local copies, waits for them, and re-layouts: 3.37 us -> 13.8 us
    all_gather x1 -> x0, waiting for transfers between devices: 9.83 us -> none  [local(): piece = lax.all_gather(tokens, 'tp', axis=1, tiled=True)]
    ppermute x0 -> x3, waiting for transfers between devices: none -> 8.13 us  [local(): lax.ppermute(held, 'tp', [(i, (i + 1) % n_dev) for i in range(n_dev)])]
    all_to_all x1, waiting for transfers between devices: 4.32 us -> 8.01 us  [local(): lax.all_to_all(send_keys, 'kv', split_axis=0, concat_axis=0, tiled=True)]
    ppermute x0 -> x3, starting transfers between devices: none -> 1.75 us  [local(): lax.ppermute(held, 'tp', [(i, (i + 1) % n_dev) for i in range(n_dev)])]
    and x1, other arithmetic: 0.47 us -> 2.12 us  [attend(): allowed = grid & (key_pos[None, :] <= query_pos[:, None])]
  transfers between devices with their start and end apart: 5 -> 7, of which waited for: 4 -> 5; matrix products, arithmetic and copies ran while one was open for 17% -> 15% of each run, Pallas kernels for 0% -> 0%
where the time goes in v1:
time: 135 us
  waiting for transfers between devices  50.8 us (38%)
  local copies, waits for them, and re-layouts  25.6 us (19%)
  matrix products  19.3 us (14%)
  starting transfers between devices  18.6 us (14%)
  between operations  13.7 us (10%)
  other arithmetic  6.76 us (5%)
    reduce_scatter x1, waiting for transfers between devices, local(): lax.psum_scatter(jnp.dot(rows, w_out, preferred_element_type=jnp.float32)...  29.4 us
    unnamed x31, local copies, waits for them, and re-layouts  13.8 us
    dot_general x3, matrix products, local(): outputs.append(jnp.dot(piece, rows, preferred_element_type=jnp.float32))  9.02 us
    ppermute x3, waiting for transfers between devices, local(): lax.ppermute(held, 'tp', [(i, (i + 1) % n_dev) for i in range(n_dev)])  8.13 us
    all_to_all x1, waiting for transfers between devices, local(): lax.all_to_all(send_keys, 'kv', split_axis=0, concat_axis=0, tiled=True)  8.01 us
    all_to_all x1, starting transfers between devices, local(): lax.all_to_all(request, 'kv', split_axis=0, concat_axis=0, tiled=True)  6.94 us
    all_to_all x1, starting transfers between devices, local(): lax.all_to_all(send_keys, 'kv', split_axis=0, concat_axis=0, tiled=True)  6 us
    all_to_all x1, waiting for transfers between devices, local(): lax.all_to_all(send_values, 'kv', split_axis=0, concat_axis=0, tiled=True)  5.21 us
  transfers between devices with their start and end apart: 7, of which 5 were waited for; matrix products, arithmetic and copies ran while one was open for 15% of the time, Pallas kernels for 0%

profile of v1, /device:TPU:0, one launch (start us, length us, event | category | flops | bytes accessed | tf_op | source)
XLA Modules:
  0.0 134.7 jit_solution(17960989357913701587)
XLA Ops:
  6.5 0.5 collective-permute-start
  7.0 0.8 fusion.41
  7.9 0.1 reshape.337
  8.0 0.1 fusion.58
  8.0 0.2 reduce_window_sum.11
  8.2 0.2 fusion.46
  8.4 0.2 select_reduce_fusion
  8.5 0.7 copy.46
  9.2 6.9 %all-to-all-start = ((s32[8,1,2]{2,1,0:T(1,128)}), s32[8,1,2]{2,1,0:T(1,128)S(1)}, u32[]{:S(2)}, u32[]{:S(2)}) async-start(s32[8,1,2]{2,1,0:T(1,128)} %copy.46), calls=%async_computation | async-start | bytes 8192 | tf_op jit(solution)/shard_map/all_to_all | solution.py:93
  16.2 0.1 copy.44
  16.2 0.1 select_n.68
  16.3 1.4 %compare_reduce_fusion = (pred[16,16]{1,0:T(8,128)(4,1)S(1)}, pred[16,16]{1,0:T(8,128)(4,1)S(1)}) fusion(s32[16,24]{1,0:T(8,128)} %param.11, s32[16]{0:T(128)S(1)} %select_n.68, s32[16]{0:T(128)S(1)} %get-tuple-element.20), kind=kLoop, calls=%fused_computation.46 | loop fusion | flops 24064 | bytes 2176 | tf_op jit(solution)/shard_map/reduce_or | solution.py:19
  17.8 0.0 collective-permute-done
  17.8 0.0 copy-start.5
  17.8 1.3 collective-permute-start.1
  19.0 0.1 iota_add_fusion
  19.1 0.1 iota_add_fusion.1
  19.2 7.4 %collective-permute-done.1 = bf16[512,512]{1,0:T(8,128)(2,1)} collective-permute-done((bf16[512,512]{1,0:T(8,128)(2,1)S(1)}, bf16[512,512]{1,0:T(8,128)(2,1)}, u32[]{:S(2)}, u32[]{:S(2)}) %collective-permute-start.1) | collective-permute-done | bytes 524320 | tf_op jit(solution)/shard_map/ppermute | solution.py:60
  26.6 0.0 collective-permute-start.2
  26.6 0.1 copy.45
  26.6 0.3 broadcast_in_dim.42
  27.0 2.1 %reshape.338 = pred[512,512]{0,1:T(8,128)(4,1)S(1)} reshape(pred[16,32,16,32]{1,0,3,2:T(8,128)(4,1)S(1)} %broadcast_in_dim.42) | data formatting | bytes 524288 | tf_op jit(solution)/shard_map/reshape | solution.py:21
  29.1 0.1 add.144
  29.2 0.1 copy.38
  29.3 0.3 broadcast_in_dim.37
  29.6 2.8 %reshape.333 = pred[512,512]{0,1:T(8,128)(4,1)} reshape(pred[16,32,16,32]{1,0,3,2:T(8,128)(4,1)S(1)} %broadcast_in_dim.37) | data formatting | bytes 524288 | tf_op jit(solution)/shard_map/reshape | solution.py:21
  32.4 0.1 add.133
  32.5 2.1 %compare_and_fusion = (pred[512,512]{0,1:T(8,128)(4,1)}, pred[512,512]{0,1:T(8,128)(4,1)S(1)}) fusion(pred[512,512]{0,1:T(8,128)(4,1)S(1)} %reshape.338, s32[512]{0:T(512)S(1)} %iota_add_fusion.2, s32[512]{0:T(512)S(1)} %add.144, pred[512,512]{0,1:T(8,128)(4,1)} %reshape.333, s32[512]{0:T(512)S(1)} %add.133), kind=kLoop, calls=%fused_computation.37 | loop fusion | flops 1048576 | bytes 1054720 | tf_op jit(solution)/shard_map/and | solution.py:28
  34.6 0.1 reshape.343
  34.7 0.8 collective-permute-done.2
  35.5 1.9 %constant_dynamic-update-slice_fusion.7 = bf16[512,4096]{1,0:T(8,128)(2,1)} fusion(bf16[512,512]{1,0:T(8,128)(2,1)} %collective-permute-done.2), kind=kLoop, calls=%fused_computation.55 | loop fusion | bytes 1048576
  37.4 1.9 %constant_dynamic-update-slice_fusion.6 = bf16[512,4096]{1,0:T(8,128)(2,1)} fusion(bf16[512,4096]{1,0:T(8,128)(2,1)} %constant_dynamic-update-slice_fusion.7, bf16[512,512]{1,0:T(8,128)(2,1)} %collective-permute-done.1), kind=kLoop, calls=%fused_computation.54 | loop fusion | bytes 1048576
  39.3 0.9 constant_dynamic-update-slice_fusion.5
  40.2 0.9 constant_dynamic-update-slice_fusion.4
  41.1 2.0 %constant_dynamic-update-slice_fusion.3 = bf16[512,4096]{1,0:T(8,128)(2,1)} fusion(bf16[512,4096]{1,0:T(8,128)(2,1)} %constant_dynamic-update-slice_fusion.4, bf16[512,512]{1,0:T(8,128)(2,1)} %collective-permute-done.2), kind=kLoop, calls=%fused_computation.51 | loop fusion | bytes 1048576
  43.1 1.9 %constant_dynamic-update-slice_fusion.2 = bf16[512,4096]{1,0:T(8,128)(2,1)} fusion(bf16[512,4096]{1,0:T(8,128)(2,1)} %constant_dynamic-update-slice_fusion.3, bf16[512,512]{1,0:T(8,128)(2,1)} %collective-permute-done.1), kind=kLoop, calls=%fused_computation.50 | loop fusion | bytes 1048576
  45.0 0.9 constant_dynamic-update-slice_fusion.1
  45.9 0.9 constant_dynamic-update-slice_fusion
  46.7 2.8 %fusion.33 = bf16[512,384]{1,0:T(8,128)(2,1)S(1)} fusion(bf16[2048,384]{1,0:T(8,128)(2,1)S(1)} %copy-done.10, bf16[512,4096]{1,0:T(8,128)(2,1)} %constant_dynamic-update-slice_fusion, s32[]{:T(128)S(6)} %select_n.64), kind=kOutput, calls=%fused_computation.36 | convolution fusion | flops 805502976 | bytes 4063236 | tf_op jit(solution)/shard_map/dot_general | solution.py:67
  49.6 0.9 copy.42
  50.5 3.2 %fusion.27 = bf16[512,384]{0,1:T(8,128)(2,1)S(1)} fusion(bf16[2048,384]{1,0:T(8,128)(2,1)} %param.7, bf16[512,4096]{1,0:T(8,128)(2,1)} %constant_dynamic-update-slice_fusion, s32[]{:T(128)S(6)} %select_n.64), kind=kOutput, calls=%fused_computation.34 | convolution fusion | flops 805502976 | bytes 4063236 | tf_op jit(solution)/shard_map/dot_general | solution.py:67
  53.7 3.0 %fusion.30 = bf16[512,384]{1,0:T(8,128)(2,1)S(1)} fusion(bf16[2048,384]{1,0:T(8,128)(2,1)S(1)} %copy-done.11, bf16[512,4096]{1,0:T(8,128)(2,1)} %constant_dynamic-update-slice_fusion, s32[]{:T(128)S(6)} %select_n.64), kind=kOutput, calls=%fused_computation.35 | convolution fusion | flops 805502976 | bytes 4063236 | tf_op jit(solution)/shard_map/dot_general | solution.py:67
  56.7 0.2 copy.39
  56.9 1.3 gather_fusion
  58.3 6.0 %all-to-all-start.1 = ((bf16[16,32,384]{2,1,0:T(8,128)(2,1)}), bf16[16,32,384]{2,1,0:T(8,128)(2,1)S(1)}, u32[]{:S(2)}, u32[]{:S(2)}) async-start(bf16[16,32,384]{2,1,0:T(8,128)(2,1)} %gather_fusion), calls=%async_computation.1 | async-start | bytes 786432 | tf_op jit(solution)/shard_map/all_to_all | solution.py:98
  64.3 1.4 %gather_fusion.1 = bf16[16,32,384]{2,1,0:T(8,128)(2,1)} fusion(bf16[16,32,384]{2,1,0:T(8,128)(2,1)S(1)} %bitcast.58, s32[1024]{0:T(1024)S(1)} %pad_clamp_fusion), kind=kCustom, calls=%fused_computation.1 | custom fusion | bytes 786496 | tf_op jit(solution)/shard_map/gather | solution.py:96
  65.7 0.8 fusion
  66.5 1.6 %copy-done.1 = f32[3,512,512]{1,2,0:T(8,128)} copy-done((f32[3,512,512]{1,2,0:T(8,128)}, f32[3,512,512]{1,2,0:T(8,128)S(1)}, u32[]{:S(2)}) %copy-start.1) | copy-done | bytes 3145752
  68.1 0.8 fusion.2
  69.0 8.0 %all-to-all-done.1 = bf16[16,32,384]{2,1,0:T(8,128)(2,1)S(1)} async-done(((bf16[16,32,384]{2,1,0:T(8,128)(2,1)}), bf16[16,32,384]{2,1,0:T(8,128)(2,1)S(1)}, u32[]{:S(2)}, u32[]{:S(2)}) %all-to-all-start.1) | async-done | bytes 393248 | tf_op jit(solution)/shard_map/all_to_all | solution.py:98
  77.0 3.6 %all-to-all-start.2 = ((bf16[16,32,384]{2,1,0:T(8,128)(2,1)}), bf16[16,32,384]{2,1,0:T(8,128)(2,1)S(1)}, u32[]{:S(2)}, u32[]{:S(2)}) async-start(bf16[16,32,384]{2,1,0:T(8,128)(2,1)} %gather_fusion.1), calls=%async_computation.2 | async-start | bytes 786432 | tf_op jit(solution)/shard_map/all_to_all | solution.py:99
  80.6 0.2 reduce-scatter.2.cloned.1.call-start
  80.8 0.1 reshape_reshape.6
  81.0 0.0 copy-start.9
  81.0 1.9 %fusion.1 = (f32[3,512]{1,0:T(4,128)S(1)}, f32[3,512,512]{1,2,0:T(8,128)S(1)}) fusion(pred[512,512]{0,1:T(8,128)(4,1)S(1)} %copy-done.7, bf16[512,3,128]{0,2,1:T(8,128)(2,1)} %bitcast.61, bf16[512,3,128]{2,1,0:T(4,128)(2,1)S(1)} %reshape_reshape.6), kind=kOutput, calls=%fused_computation.8 | convolution fusion | flops 203684352 | bytes 4200448 | tf_op jit(solution)/shard_map/qhd,khd->hqk/dot_general | solution.py:32
  82.9 1.7 %copy-done.3 = f32[3,512,512]{1,2,0:T(8,128)} copy-done((f32[3,512,512]{1,2,0:T(8,128)}, f32[3,512,512]{1,2,0:T(8,128)S(1)}, u32[]{:S(2)}) %copy-start.3) | copy-done | bytes 3145752
  84.6 0.8 fusion.4
  85.5 1.9 %fusion.24 = f32[512,3,128]{0,2,1:T(8,128)} fusion(bf16[512,3,128]{0,2,1:T(8,128)(2,1)S(1)} %bitcast.62, f32[3,512,512]{1,2,0:T(8,128)S(1)} %copy-done.2, f32[3,512]{1,0:T(4,128)S(1)} %get-tuple-element.16, pred[512,512]{0,1:T(8,128)(4,1)S(1)} %get-tuple-element.13, f32[512,3]{0,1:T(4,128)S(1)} %get-tuple-element.9), kind=kOutput, calls=%fused_computation.31 | convolution fusion | flops 204668928 | bytes 4599808 | tf_op jit(solution)/shard_map/hqk,khd->hqd/dot_general | solution.py:39
  87.3 5.2 %all-to-all-done.2 = bf16[16,32,384]{2,1,0:T(8,128)(2,1)S(1)} async-done(((bf16[16,32,384]{2,1,0:T(8,128)(2,1)}), bf16[16,32,384]{2,1,0:T(8,128)(2,1)S(1)}, u32[]{:S(2)}, u32[]{:S(2)}) %all-to-all-start.2) | async-done | bytes 393248 | tf_op jit(solution)/shard_map/all_to_all | solution.py:99
  92.5 0.1 reshape_reshape.7
  92.6 3.1 %fusion.37 = bf16[512,3,128]{0,2,1:T(8,128)(2,1)S(1)} fusion(f32[512,3,128]{0,2,1:T(8,128)} %fusion.24, f32[3,512,512]{1,2,0:T(8,128)} %copy-done.3, f32[3,512]{1,0:T(4,128)S(1)} %get-tuple-element.18, pred[512,512]{0,1:T(8,128)(4,1)S(1)} %copy-done.7, bf16[512,3,128]{2,1,0:T(4,128)(2,1)S(1)} %reshape_reshape.7, f32[512,3]{0,1:T(4,128)S(1)} %get-tuple-element.7, ...), kind=kOutput, calls=%fused_computation.40 | convolution fusion | flops 205258752 | bytes 4999168 | tf_op jit(solution)/shard_map/hqk,khd->hqd/dot_general | solution.py:39
  95.7 2.7 %convolution_convert_fusion = bf16[512,2048]{1,0:T(8,128)(2,1)} fusion(bf16[512,384]{0,1:T(8,128)(2,1)S(1)} %bitcast.63, bf16[384,2048]{1,0:T(8,128)(2,1)S(1)} %copy-done), kind=kOutput, calls=%fused_computation.6 | convolution fusion | flops 806354944 | bytes 4063232 | tf_op jit(solution)/shard_map/dot_general | solution.py:115
  98.4 0.0 reduce-scatter.2.cloned.1.call-update
  98.4 29.4 %reduce-scatter.2.cloned.1.call-done = bf16[128,2048]{1,0:T(8,128)(2,1)} async-done(((bf16[512,2048]{1,0:T(8,128)(2,1)}), bf16[128,2048]{1,0:T(8,128)(2,1)}) %reduce-scatter.2.cloned.1.call-update) | async-done | bytes 524304 | tf_op jit(solution)/shard_map/reduce_scatter | solution.py:114
  (35 shorter events, 0.1 us)
Async XLA Ops:
  6.5 89.2 %copy-start = (bf16[384,2048]{1,0:T(8,128)(2,1)S(1)}, bf16[384,2048]{1,0:T(8,128)(2,1)}, u32[]{:S(2)}) copy-start(bf16[384,2048]{1,0:T(8,128)(2,1)} %param.10) | copy-start | bytes 4718596
  6.5 11.2 %collective-permute-start = (bf16[512,512]{1,0:T(8,128)(2,1)}, bf16[512,512]{1,0:T(8,128)(2,1)S(1)}, u32[]{:S(2)}, u32[]{:S(2)}) collective-permute-start(bf16[512,512]{1,0:T(8,128)(2,1)} %param.6), channel_id=1, source_target_pairs={{0,1},{1,2},{2,3},{3,0},{4,5},{5,6},{6,7},{7,4},{8,9},{9,10},{10,1... | collective-permute-start | bytes 1572872 | tf_op jit(solution)/shard_map/ppermute | solution.py:60
  9.2 25.4 %all-to-all-start = ((s32[8,1,2]{2,1,0:T(1,128)}), s32[8,1,2]{2,1,0:T(1,128)S(1)}, u32[]{:S(2)}, u32[]{:S(2)}) async-start(s32[8,1,2]{2,1,0:T(1,128)} %copy.46), calls=%async_computation | async-start | bytes 8192 | tf_op jit(solution)/shard_map/all_to_all | solution.py:93
  17.8 8.8 %copy-start.5 = (bf16[512,512]{1,0:T(8,128)(2,1)}, bf16[512,512]{1,0:T(8,128)(2,1)S(1)}, u32[]{:S(2)}) copy-start(bf16[512,512]{1,0:T(8,128)(2,1)S(1)} %collective-permute-done) | copy-start | bytes 1572868
  17.8 8.8 %collective-permute-start.1 = (bf16[512,512]{1,0:T(8,128)(2,1)S(1)}, bf16[512,512]{1,0:T(8,128)(2,1)}, u32[]{:S(2)}, u32[]{:S(2)}) collective-permute-start(bf16[512,512]{1,0:T(8,128)(2,1)S(1)} %collective-permute-done), channel_id=1, source_target_pairs={{0,1},{1,2},{2,3},{3,0},{4,5},{5,6},{6,7},{7,4},{8,9},{9,10},{10,1... | collective-permute-start | bytes 1572872 | tf_op jit(solution)/shard_map/ppermute | solution.py:60
  26.6 8.9 %collective-permute-start.2 = (bf16[512,512]{1,0:T(8,128)(2,1)}, bf16[512,512]{1,0:T(8,128)(2,1)}, u32[]{:S(2)}, u32[]{:S(2)}) collective-permute-start(bf16[512,512]{1,0:T(8,128)(2,1)} %collective-permute-done.1), channel_id=1, source_target_pairs={{0,1},{1,2},{2,3},{3,0},{4,5},{5,6},{6,7},{7,4},{8,9},{9,10},{10,1... | collective-permute-start | bytes 1572872 | tf_op jit(solution)/shard_map/ppermute | solution.py:60
  29.3 10.9 %copy-start.4 = (bf16[512,512]{1,0:T(8,128)(2,1)S(1)}, bf16[512,512]{1,0:T(8,128)(2,1)}, u32[]{:S(2)}) copy-start(bf16[512,512]{1,0:T(8,128)(2,1)} %param.6) | copy-start | bytes 1572868
  32.4 6.9 %copy-start.6 = (bf16[512,512]{1,0:T(8,128)(2,1)S(1)}, bf16[512,512]{1,0:T(8,128)(2,1)}, u32[]{:S(2)}) copy-start(bf16[512,512]{1,0:T(8,128)(2,1)} %copy-done.5) | copy-start | bytes 1572868
  39.3 7.4 %copy-start.10 = (bf16[2048,384]{1,0:T(8,128)(2,1)S(1)}, bf16[2048,384]{1,0:T(8,128)(2,1)}, u32[]{:S(2)}) copy-start(bf16[2048,384]{1,0:T(8,128)(2,1)} %param.9) | copy-start | bytes 4718596
  50.5 3.2 %copy-start.11 = (bf16[2048,384]{1,0:T(8,128)(2,1)S(1)}, bf16[2048,384]{1,0:T(8,128)(2,1)}, u32[]{:S(2)}) copy-start(bf16[2048,384]{1,0:T(8,128)(2,1)} %param.8) | copy-start | bytes 4718596
  53.7 26.9 %copy-start.8 = (bf16[512,384]{0,1:T(8,128)(2,1)}, bf16[512,384]{0,1:T(8,128)(2,1)S(1)}, u32[]{:S(2)}) copy-start(bf16[512,384]{0,1:T(8,128)(2,1)S(1)} %fusion.27) | copy-start | bytes 1179652
  58.3 18.7 %all-to-all-start.1 = ((bf16[16,32,384]{2,1,0:T(8,128)(2,1)}), bf16[16,32,384]{2,1,0:T(8,128)(2,1)S(1)}, u32[]{:S(2)}, u32[]{:S(2)}) async-start(bf16[16,32,384]{2,1,0:T(8,128)(2,1)} %gather_fusion), calls=%async_computation.1 | async-start | bytes 786432 | tf_op jit(solution)/shard_map/all_to_all | solution.py:98
  66.5 1.7 %copy-start.1 = (f32[3,512,512]{1,2,0:T(8,128)}, f32[3,512,512]{1,2,0:T(8,128)S(1)}, u32[]{:S(2)}) copy-start(f32[3,512,512]{1,2,0:T(8,128)S(1)} %get-tuple-element.17) | copy-start | bytes 9437188
  66.5 14.5 %copy-start.7 = (pred[512,512]{0,1:T(8,128)(4,1)S(1)}, pred[512,512]{0,1:T(8,128)(4,1)}, u32[]{:S(2)}) copy-start(pred[512,512]{0,1:T(8,128)(4,1)} %get-tuple-element.12) | copy-start | bytes 786436
  77.0 15.6 %all-to-all-start.2 = ((bf16[16,32,384]{2,1,0:T(8,128)(2,1)}), bf16[16,32,384]{2,1,0:T(8,128)(2,1)S(1)}, u32[]{:S(2)}, u32[]{:S(2)}) async-start(bf16[16,32,384]{2,1,0:T(8,128)(2,1)} %gather_fusion.1), calls=%async_computation.2 | async-start | bytes 786432 | tf_op jit(solution)/shard_map/all_to_all | solution.py:99
  80.6 47.2 %reduce-scatter.2.cloned.1.call-start = ((), (), s32[]{:S(2)}) async-start(), calls=%async_computation.4 | async-start | bytes 2621440 | tf_op jit(solution)/shard_map/reduce_scatter | solution.py:114
  81.0 4.5 %copy-start.2 = (f32[3,512,512]{1,2,0:T(8,128)S(1)}, f32[3,512,512]{1,2,0:T(8,128)}, u32[]{:S(2)}) copy-start(f32[3,512,512]{1,2,0:T(8,128)} %copy-done.1) | copy-start | bytes 9437188
  81.0 4.5 %copy-start.9 = (bf16[512,384]{0,1:T(8,128)(2,1)S(1)}, bf16[512,384]{0,1:T(8,128)(2,1)}, u32[]{:S(2)}) copy-start(bf16[512,384]{0,1:T(8,128)(2,1)} %copy.42) | copy-start | bytes 1179652
  82.9 1.7 %copy-start.3 = (f32[3,512,512]{1,2,0:T(8,128)}, f32[3,512,512]{1,2,0:T(8,128)S(1)}, u32[]{:S(2)}) copy-start(f32[3,512,512]{1,2,0:T(8,128)S(1)} %get-tuple-element.19) | copy-start | bytes 9437188
Sparse Core Ops, SparseCore 0:
  98.5 29.2 reduce-scatter.1
